TPU v7x, 32 devices: a whole 2x2x4 slice. The times are simulated.
32 devices in a mesh: sp: 8 (over z, y), dp: 4 (over x, core).
Axes of the slice: x: 2, y: 2, z: 4, core: 2. Of those that a mesh axis runs over, the one named last changes fastest.
Arguments:
- residual: bfloat16 [4, 1024, 2048], P('dp', 'sp'), may hold values from -6 to 6
- head_input: bfloat16 [4, 1024, 2048], P('dp', 'sp'), may hold values from -6 to 6
- gate_input: bfloat16 [4, 1024, 2048], P('dp', 'sp'), may hold values from -6 to 6
- b_input: bfloat16 [4, 1024, 1024], P('dp', 'sp'), may hold values from -6 to 6
- c_input: bfloat16 [4, 1024, 1024], P('dp', 'sp'), may hold values from -6 to 6
- step_input: bfloat16 [4, 1024, 32], P('dp', 'sp'), may hold values from -4.8 to 4.8
- conv_weight: bfloat16 [4, 2048], replicated, may hold values from -3 to 3
- conv_b_weight: bfloat16 [4, 1024], replicated, may hold values from -3 to 3
- conv_c_weight: bfloat16 [4, 1024], replicated, may hold values from -3 to 3
- step_bias: float32 [32], replicated, may hold values from -1 to 1
- decay_log: float32 [32], replicated, may hold values from -9.92 to -2.99
- skip: float32 [32], replicated, may hold values from 0.5 to 1.5
- norm_gain: float32 [2048], replicated, may hold values from 0.1 to 1.9
- out_weight: bfloat16 [2048, 2048], P('dp'), may hold values from -0.125 to 0.125
- ffn_gain: float32 [2048], replicated, may hold values from 0.1 to 1.9
- shared_gate: bfloat16 [2048, 512], replicated, may hold values from -0.125 to 0.125
- shared_up: bfloat16 [2048, 512], replicated, may hold values from -0.125 to 0.125
- shared_down: bfloat16 [512, 2048], replicated, may hold values from -0.25 to 0.25
- expert_gate: bfloat16 [32, 2048, 512], P(('sp', 'dp')), may hold values from -0.125 to 0.125
- expert_up: bfloat16 [32, 2048, 512], P(('sp', 'dp')), may hold values from -0.125 to 0.125
- expert_down: bfloat16 [32, 512, 2048], P(('sp', 'dp')), may hold values from -0.25 to 0.25
- routes: int32 [4, 1024, 2], P('dp', 'sp'), may hold values from 0 to 31, all different within a row; in each aligned block of 128 rows (0 to 127, 128 to 255, ..., all dimensions but the last counted through in order) at most 16 rows name the same one
- route_weights: float32 [4, 1024, 2], P('dp', 'sp'), may hold values from 0.25 to 1.25
Outputs:
- layer_out: bfloat16 [4, 1024, 2048], P('dp', 'sp')
Inputs may be any that keep to these rules, and one draw needn't show every extreme that they name: `routes`: each token names 2 different experts; among the rows of one device no expert is named more than 16 times, a bound that some block reaches.
All inputs are finite; a program needn't handle non-finite values.
Results may differ from a plain program's by a relative error of at most 0.015.
Values may be sent and summed in bfloat16 or wider, within the bound.
A program may use at most 128 MiB of HBM per device.

v0:
```python
import jax
import jax.numpy as jnp
import numpy as np
from jax import lax
from jax.sharding import PartitionSpec as P

D = 2048
HEADS = 32
HEAD_DIM = 64
GROUPS = 8
STATE = 128
CONV_K = 4
BLOCK = 128
TOP_K = 2
INNER = 2048


EPS = 1e-06
HIGH = lax.Precision.HIGHEST


def conv_silu(padded, weight, length):
    total = jnp.zeros((length, padded.shape[1]), jnp.float32)
    for tap in range(weight.shape[0]):
        total = total + padded[tap : tap + length].astype(jnp.float32) * weight[tap].astype(
            jnp.float32
        )
    return jax.nn.silu(total)


def block_scan(xs, step, rate, bmat, cmat, block, init):
    length, heads, width = xs.shape
    count = length // block
    logs = (step * rate[None, :]).reshape(count, block, heads)
    weighted = (xs * step[:, :, None]).reshape(count, block, heads, width)
    bb = bmat.reshape(count, block, heads, -1)
    cc = cmat.reshape(count, block, heads, -1)
    cum = jnp.cumsum(logs, axis=1)
    lower = jnp.tril(jnp.ones((block, block), dtype=bool))[None, :, :, None]
    diff = cum[:, :, None, :] - cum[:, None, :, :]
    decay = jnp.where(lower, jnp.exp(jnp.where(lower, diff, 0.0)), 0.0)
    scores = jnp.einsum("clhn,cshn->clsh", cc, bb, precision=HIGH) * decay
    inner = jnp.einsum("clsh,cshp->clhp", scores, weighted, precision=HIGH)
    to_end = jnp.exp(cum[:, -1:, :] - cum)
    states = jnp.einsum("cshn,cshp->chpn", bb * to_end[..., None], weighted, precision=HIGH)
    totals = jnp.exp(cum[:, -1, :])

    def advance(carry, item):
        fresh, factor = item
        return (carry * factor[:, None, None] + fresh, carry)

    last, before = lax.scan(advance, init, (states, totals))
    outer = jnp.einsum("clhn,chpn->clhp", cc * jnp.exp(cum)[..., None], before, precision=HIGH)
    return ((inner + outer).reshape(length, heads, width), last)


def serve_experts(arrived, gate_w, up_w, down_w):
    local = gate_w.shape[0]
    shaped = arrived.reshape(-1, local, arrived.shape[1], arrived.shape[2])
    gate = jnp.einsum("aenc,ecf->aenf", shaped, gate_w, preferred_element_type=jnp.float32)
    up = jnp.einsum("aenc,ecf->aenf", shaped, up_w, preferred_element_type=jnp.float32)
    hidden = (jax.nn.silu(gate) * up).astype(jnp.bfloat16)
    done = jnp.einsum("aenf,efc->aenc", hidden, down_w, preferred_element_type=jnp.float32).astype(
        jnp.bfloat16
    )
    return done.reshape(arrived.shape)


def body(
    residual,
    head_input,
    gate_input,
    b_input,
    c_input,
    step_input,
    conv_weight,
    conv_b_weight,
    conv_c_weight,
    step_bias,
    decay_log,
    skip,
    norm_gain,
    out_weight,
    ffn_gain,
    shared_gate,
    shared_up,
    shared_down,
    expert_gate,
    expert_up,
    expert_down,
    routes,
    route_weights,
):
    tokens = head_input.shape[1]
    x_rows = head_input[0]
    b_rows = b_input[0]
    c_rows = c_input[0]
    step_rows = step_input[0]
    per_group = HEADS // GROUPS
    ways = lax.axis_size("sp")
    place = lax.axis_index("sp")
    local = HEADS // ways
    width = local * HEAD_DIM
    targets = np.arange(ways) * local // per_group
    paired = jnp.concatenate(
        [b_rows.reshape(tokens, GROUPS, STATE), c_rows.reshape(tokens, GROUPS, STATE)], axis=2
    )
    outgoing = (
        x_rows.reshape(tokens, ways, width),
        paired[:, targets],
        step_rows.reshape(tokens, ways, local),
    )
    got_x, got_pair, got_step = (
        lax.all_to_all(outgoing[0], "sp", split_axis=1, concat_axis=0, tiled=True),
        lax.all_to_all(outgoing[1], "sp", split_axis=1, concat_axis=0, tiled=True),
        lax.all_to_all(outgoing[2], "sp", split_axis=1, concat_axis=0, tiled=True),
    )
    length = got_x.shape[0]
    group = place * local // per_group
    taps = jnp.concatenate(
        [
            lax.dynamic_slice_in_dim(conv_weight, place * width, width, 1),
            lax.dynamic_slice_in_dim(conv_b_weight, group * STATE, STATE, 1),
            lax.dynamic_slice_in_dim(conv_c_weight, group * STATE, STATE, 1),
        ],
        axis=1,
    )
    rows = jnp.concatenate(
        [got_x.reshape(length, width), got_pair.reshape(length, 2 * STATE)], axis=1
    )
    act = conv_silu(jnp.pad(rows, ((CONV_K - 1, 0), (0, 0))), taps, length)
    xs = act[:, :width].reshape(length, local, HEAD_DIM)
    bm = jnp.broadcast_to(act[:, width : width + STATE][:, None, :], (length, local, STATE))
    cm = jnp.broadcast_to(act[:, width + STATE :][:, None, :], (length, local, STATE))
    step = jax.nn.softplus(
        got_step.reshape(length, local).astype(jnp.float32)
        + lax.dynamic_slice_in_dim(step_bias, place * local, local, 0)[None, :]
    )
    rate = -jnp.exp(lax.dynamic_slice_in_dim(decay_log, place * local, local, 0))
    skip_local = lax.dynamic_slice_in_dim(skip, place * local, local, 0)
    y, _ = block_scan(
        xs, step, rate, bm, cm, BLOCK, jnp.zeros((local, HEAD_DIM, STATE), jnp.float32)
    )
    y = (y + skip_local[None, :, None] * xs).astype(jnp.bfloat16).reshape(ways, tokens, width)
    scanned = lax.all_to_all(y, "sp", split_axis=0, concat_axis=2, tiled=True).reshape(
        tokens, INNER
    )
    gated = (scanned.astype(jnp.float32) * jax.nn.silu(gate_input[0].astype(jnp.float32))).reshape(
        tokens, GROUPS, INNER // GROUPS
    )
    gated = gated * lax.rsqrt(jnp.mean(gated * gated, axis=2, keepdims=True) + EPS)
    normed = (gated.reshape(tokens, INNER) * norm_gain[None, :]).astype(jnp.bfloat16)
    projected = jnp.dot(
        normed,
        lax.all_gather(out_weight, "dp", axis=0, tiled=True),
        preferred_element_type=jnp.float32,
    )
    mixed = (residual[0].astype(jnp.float32) + projected).astype(jnp.bfloat16)
    mixed_f = mixed.astype(jnp.float32)
    expert_in = (
        mixed_f
        * lax.rsqrt(jnp.mean(mixed_f * mixed_f, axis=1, keepdims=True) + EPS)
        * ffn_gain[None, :]
    ).astype(jnp.bfloat16)
    shared_hidden = (
        jax.nn.silu(jnp.dot(expert_in, shared_gate, preferred_element_type=jnp.float32))
        * jnp.dot(expert_in, shared_up, preferred_element_type=jnp.float32)
    ).astype(jnp.bfloat16)
    shared = jnp.dot(shared_hidden, shared_down, preferred_element_type=jnp.float32)
    ways_sp = lax.axis_size("sp")
    ways_dp = lax.axis_size("dp")
    experts = ways_sp * ways_dp * expert_gate.shape[0]
    slots = 2 * tokens * TOP_K // experts
    chosen = routes[0].reshape(-1)
    pairs = chosen.shape[0]
    onehot = (chosen[:, None] == jnp.arange(experts, dtype=jnp.int32)[None, :]).astype(jnp.int32)
    position = jnp.sum((jnp.cumsum(onehot, axis=0) - onehot) * onehot, axis=1)
    target = chosen * slots + position
    owner = jnp.arange(pairs, dtype=jnp.int32) // TOP_K
    outgoing = jnp.zeros((experts * slots, D), jnp.bfloat16).at[target].set(expert_in[owner])
    outgoing = outgoing.reshape(experts, slots, D)
    done = serve_experts(
        lax.all_to_all(outgoing, ("sp", "dp"), split_axis=0, concat_axis=0, tiled=True),
        expert_gate,
        expert_up,
        expert_down,
    )
    returned = lax.all_to_all(done, ("sp", "dp"), split_axis=0, concat_axis=0, tiled=True)
    pair_out = returned.reshape(experts * slots, D)[target]
    routed = jnp.sum(
        pair_out.reshape(tokens, TOP_K, D).astype(jnp.float32) * route_weights[0][:, :, None],
        axis=1,
    )
    return (mixed_f + shared + routed).astype(jnp.bfloat16)[None]


def solution(mesh):
    return jax.shard_map(
        body,
        mesh=mesh,
        in_specs=(
            P("dp", "sp", None),
            P("dp", "sp", None),
            P("dp", "sp", None),
            P("dp", "sp", None),
            P("dp", "sp", None),
            P("dp", "sp", None),
            P(),
            P(),
            P(),
            P(),
            P(),
            P(),
            P(),
            P("dp", None),
            P(),
            P(),
            P(),
            P(),
            P(("sp", "dp"), None, None),
            P(("sp", "dp"), None, None),
            P(("sp", "dp"), None, None),
            P("dp", "sp", None),
            P("dp", "sp", None),
        ),
        out_specs=P("dp", "sp", None),
        check_vma=False,
    )
```

profile of v0, /device:TPU:0, one launch (start us, length us, event | category | flops | bytes accessed | tf_op | source)
XLA Modules:
  0.0 292.4 jit_solution(8568359432632893805)
XLA Ops:
  7.3 7.5 %all-to-all-start.2 = ((bf16[128,8,4]{0,2,1:T(4,128)(2,1)}), bf16[128,8,4]{0,2,1:T(4,128)(2,1)S(1)}, u32[]{:S(2)}, u32[]{:S(2)}) async-start(bf16[128,8,4]{0,2,1:T(4,128)(2,1)} %bitcast.15), calls=%async_computation.2 | async-start | bytes 16384 | tf_op jit(solution)/shard_map/all_to_all | solution.py:116
  15.8 5.5 %all-to-all-done.2 = bf16[128,8,4]{0,2,1:T(4,128)(2,1)S(1)} async-done(((bf16[128,8,4]{0,2,1:T(4,128)(2,1)}), bf16[128,8,4]{0,2,1:T(4,128)(2,1)S(1)}, u32[]{:S(2)}, u32[]{:S(2)}) %all-to-all-start.2) | async-done | bytes 8224 | tf_op jit(solution)/shard_map/all_to_all | solution.py:116
  21.2 3.5 %all-to-all-start = ((bf16[128,8,256]{0,2,1:T(8,128)(2,1)}), bf16[128,8,256]{0,2,1:T(8,128)(2,1)S(1)}, u32[]{:S(2)}, u32[]{:S(2)}) async-start(bf16[128,8,256]{0,2,1:T(8,128)(2,1)} %bitcast.1), calls=%async_computation | async-start | bytes 1048576 | tf_op jit(solution)/shard_map/all_to_all | solution.py:114
  35.2 2.8 all-to-all-done
  38.0 4.1 %all-to-all-start.1 = ((bf16[128,8,256]{2,0,1:T(8,128)(2,1)}), bf16[128,8,256]{2,0,1:T(8,128)(2,1)}, u32[]{:S(2)}, u32[]{:S(2)}) async-start(bf16[128,8,256]{2,0,1:T(8,128)(2,1)} %bitcast.7), calls=%async_computation.1 | async-start | bytes 1048576 | tf_op jit(solution)/shard_map/all_to_all | solution.py:115
  42.5 23.3 %fusion.88 = f32[8,128,4]{2,0,1:T(8,128)S(1)} fusion(f32[8,128,4]{2,0,1:T(8,128)S(1)} %copy.122), kind=kOutput, calls=%fused_computation.132 | output fusion | flops 520192 | bytes 32768 | tf_op jit(solution)/shard_map/jit(cumsum)/reduce_window_sum | solution.py:38
  77.4 3.2 %fusion.14 = f32[8,4,64,128]{3,2,1,0:T(8,128)} fusion(f32[8,128,4]{1,2,0:T(4,128)S(1)} %copy.129, f32[8,128,128]{2,1,0:T(8,128)S(1)} %bitcast.211, f32[8,128,4,64]{1,0,3,2:T(8,128)S(1)} %broadcast_multiply_fusion), kind=kOutput, calls=%fused_computation.26 | convolution fusion | flops 403177472 | bytes 2637824 | tf_op jit(solution)/shard_map/cshn,cshp->chpn/dot_general | solution.py:45
  80.5 4.4 %fusion.57 = f32[8,4,128,128]{3,2,1,0:T(8,128)S(1)} fusion(f32[8,128,128]{2,1,0:T(8,128)S(1)} %bitcast.209, f32[8,128,128]{2,1,0:T(8,128)S(1)} %bitcast.212), kind=kOutput, calls=%fused_computation.68 | convolution fusion | flops 805306368 | bytes 3145728 | tf_op jit(solution)/shard_map/clhn,cshn->clsh/dot_general | solution.py:42
  85.0 3.5 %fusion.11 = f32[8,4,64,128]{3,2,1,0:T(8,128)} fusion(f32[8,4,128,128]{3,2,1,0:T(8,128)S(1)} %fusion.57, f32[8,128,4]{1,2,0:T(4,128)S(1)} %copy.123, pred[128,128]{0,1:T(8,128)(4,1)S(1)} %iota_compare_fusion, f32[8,128,4,64]{1,0,3,2:T(8,128)S(1)} %broadcast_multiply_fusion), kind=kOutput, calls=%fused_computation.22 | convolution fusion | flops 404750336 | bytes 4227072 | tf_op jit(solution)/shard_map/clsh,cshp->clhp/dot_general | solution.py:43
  88.5 13.5 %while.13 = (s32[]{:T(128)}, f32[4,64,128]{2,1,0:T(8,128)S(1)}, f32[8,4,64,128]{3,2,1,0:T(8,128)}, f32[8,4]{1,0:T(8,128)S(1)}, f32[8,4,64,128]{3,2,1,0:T(8,128)}, /*index=5*/s32[]{:T(128)}, s32[]{:T(128)}) while((s32[]{:T(128)}, f32[4,64,128]{2,1,0:T(8,128)S(1)}, f32[8,4,64,128]{3,2,1,0:T(8,128)}, f32[8,4]{1,0:T(8,128)S(1)}, ...), condition=%wide.region_2.3_spmd.clone, body=%wide.region_1.2_spmd.clone.sunk | while | flops 131075 | bytes 656016 | solution.py:52
  102.0 7.0 %fusion.20 = f32[8,4,64,128]{3,2,1,0:T(8,128)} fusion(f32[8,4,64,128]{3,2,1,0:T(8,128)} %fusion.11, f32[8,4,64,128]{3,2,1,0:T(8,128)} %get-tuple-element.32, f32[8,128,4]{1,2,0:T(4,128)S(1)} %copy.132, f32[8,128,128]{2,1,0:T(8,128)} %bitcast.210), kind=kOutput, calls=%fused_computation.33 | convolution fusion | flops 403439616 | bytes 3686400 | tf_op jit(solution)/shard_map/clhn,chpn->clhp/dot_general | solution.py:53
  113.7 6.0 %all-to-all-start.3 = ((bf16[8,128,256]{2,1,0:T(8,128)(2,1)}), bf16[8,128,256]{2,1,0:T(8,128)(2,1)S(1)}, u32[]{:S(2)}, u32[]{:S(2)}) async-start(bf16[8,128,256]{2,1,0:T(8,128)(2,1)} %add_convert_fusion), calls=%async_computation.3 | async-start | bytes 1048576 | tf_op jit(solution)/shard_map/all_to_all | solution.py:145
  123.7 8.8 %all-to-all-done.3 = bf16[8,128,256]{2,1,0:T(8,128)(2,1)S(1)} async-done(((bf16[8,128,256]{2,1,0:T(8,128)(2,1)}), bf16[8,128,256]{2,1,0:T(8,128)(2,1)S(1)}, u32[]{:S(2)}, u32[]{:S(2)}) %all-to-all-start.3) | async-done | bytes 524320 | tf_op jit(solution)/shard_map/all_to_all | solution.py:145
  133.7 2.5 copy.134
  139.2 4.9 %multiply_reduce_fusion.1 = (f32[128]{0:T(128)S(1)}, f32[128,2048]{1,0:T(8,128)S(1)}) fusion(bf16[128,2048]{0,1:T(8,128)(2,1)} %fusion.43, bf16[2048,2048]{1,0:T(8,128)(2,1)} %all-gather.2.cloned.1.call-done, bf16[1,128,2048]{2,1,0:T(8,128)(2,1)} %param.27), kind=kOutput, calls=%fused_computation.60 | convolution fusion | flops 1075314560 | bytes 10486272 | tf_op jit(solution)/shard_map/dot_general | solution.py:153
  145.1 7.2 %scatter_custom_fusion = bf16[512,2048]{1,0:T(8,128)(2,1)} fusion(s32[256]{0:T(256)S(1)} %bitcast.225, bf16[128,2048]{1,0:T(8,128)(2,1)} %multiply_convert_fusion, s32[1024]{0:T(1024)S(1)} %pad_clamp_fusion.1, bf16[]{:T(256)} %constant.86.clone.1), kind=kCustom, calls=%fused_computation.56 | custom fusion | bytes 2097664 | tf_op jit(solution)/shard_map/scatter | solution.py:180
  152.3 52.4 %all_to_all.58 = bf16[32,16,2048]{2,1,0:T(8,128)(2,1)S(1)} all-to-all(bf16[32,16,2048]{2,1,0:T(8,128)(2,1)} %bitcast.207), channel_id=1, replica_groups=mesh['sp'=8,'dp'=4] {'sp','dp'}, dimensions={0} | all-to-all | bytes 4194304 | tf_op jit(solution)/shard_map/all_to_all | solution.py:183
  208.2 6.2 %convolution_convert_fusion = bf16[32,16,2048]{2,1,0:T(8,128)(2,1)} fusion(bf16[1,512,2048]{2,1,0:T(8,128)(2,1)S(1)} %copy-done, bf16[32,16,2048]{2,1,0:T(8,128)(2,1)} %copy-done.5, bf16[1,2048,512]{2,1,0:T(8,128)(2,1)} %param.46, f32[32,1,16,512]{3,2,0,1:T(8,128)} %fusion.23), kind=kOutput, calls=%fused_computation.8 | convolution fusion | flops 2150105088 | bytes 9437184 | tf_op jit(solution)/shard_map/aenf,efc->aenc/dot_general | solution.py:63
  214.5 3.8 %all-to-all-start.5 = ((bf16[32,16,2048]{2,1,0:T(8,128)(2,1)}), bf16[32,16,2048]{2,1,0:T(8,128)(2,1)}, u32[]{:S(2)}, u32[]{:S(2)}) async-start(bf16[32,16,2048]{2,1,0:T(8,128)(2,1)} %convolution_convert_fusion), calls=%async_computation.5 | async-start | bytes 4194304 | tf_op jit(solution)/shard_map/all_to_all | solution.py:188
  220.6 46.4 %all-to-all-done.5 = bf16[32,16,2048]{2,1,0:T(8,128)(2,1)} async-done(((bf16[32,16,2048]{2,1,0:T(8,128)(2,1)}), bf16[32,16,2048]{2,1,0:T(8,128)(2,1)}, u32[]{:S(2)}, u32[]{:S(2)}) %all-to-all-start.5) | async-done | bytes 2097184 | tf_op jit(solution)/shard_map/all_to_all | solution.py:188
  267.0 5.2 %gather_fusion.1 = bf16[256,2048]{1,0:T(8,128)(2,1)} fusion(bf16[512,2048]{1,0:T(8,128)(2,1)} %bitcast.54, s32[1024]{0:T(1024)S(1)} %pad_clamp_fusion), kind=kCustom, calls=%fused_computation.2 | custom fusion | bytes 2098176 | tf_op jit(solution)/shard_map/gather | solution.py:189
  272.2 3.4 %reshape.277 = f32[128,2,2048]{2,1,0:T(2,128)} reshape(bf16[256,2048]{1,0:T(8,128)(2,1)} %gather_fusion.1) | data formatting | bytes 3145728 | tf_op jit(solution)/shard_map/convert_element_type | solution.py:191
  275.5 5.7 %multiply_reduce_fusion = f32[128,2048]{1,0:T(8,128)} fusion(f32[128,2,2048]{2,1,0:T(2,128)} %reshape.277, f32[128,2]{1,0:T(8,128)S(1)} %copy.142), kind=kLoop, calls=%fused_computation.23 | loop fusion | flops 786432 | bytes 3146752 | tf_op jit(solution)/shard_map/reduce_sum | solution.py:190
  281.3 4.3 %fusion.5 = bf16[1,128,2048]{2,1,0:T(8,128)(2,1)} fusion(f32[128,2048]{1,0:T(8,128)} %multiply_reduce_fusion, f32[128,2048]{1,0:T(8,128)S(1)} %get-tuple-element.97, bf16[512,2048]{1,0:T(8,128)(2,1)} %param.44, bf16[128,2048]{1,0:T(8,128)(2,1)} %multiply_convert_fusion, bf16[2048,512]{1,0:T(8,128)(2,1)} %param.43, f32[128,512]{1,0:T(8,128)S(1)} %fusion.89), kind=kOutput, calls=%fused_computation.15 | convolution fusion | flops 538050560 | bytes 7602176 | tf_op jit(solution)/shard_map/dot_general | solution.py:169
  (135 shorter events, 56.7 us)
Async XLA Ops:
  6.5 201.7 %copy-start = (bf16[1,512,2048]{2,1,0:T(8,128)(2,1)S(1)}, bf16[1,512,2048]{2,1,0:T(8,128)(2,1)}, u32[]{:S(2)}) copy-start(bf16[1,512,2048]{2,1,0:T(8,128)(2,1)} %param.47) | copy-start | bytes 6291460
  6.5 8.2 %copy-start.9 = (bf16[1,128,2048]{2,1,0:T(8,128)(2,1)S(1)}, bf16[1,128,2048]{2,1,0:T(8,128)(2,1)}, u32[]{:S(2)}) copy-start(bf16[1,128,2048]{2,1,0:T(8,128)(2,1)} %param.28) | copy-start | bytes 1572868
  6.5 18.3 %copy-start.10 = (bf16[1,128,1024]{2,1,0:T(8,128)(2,1)S(1)}, bf16[1,128,1024]{2,1,0:T(8,128)(2,1)}, u32[]{:S(2)}) copy-start(bf16[1,128,1024]{2,1,0:T(8,128)(2,1)} %param.30) | copy-start | bytes 786436
  6.5 132.6 %all-gather.2.cloned.1.call-start = ((), (), s32[]{:S(2)}) async-start(), calls=%async_computation.6 | async-start | bytes 10485760 | tf_op jit(solution)/shard_map/all_gather | solution.py:155
  7.3 14.0 %all-to-all-start.2 = ((bf16[128,8,4]{0,2,1:T(4,128)(2,1)}), bf16[128,8,4]{0,2,1:T(4,128)(2,1)S(1)}, u32[]{:S(2)}, u32[]{:S(2)}) async-start(bf16[128,8,4]{0,2,1:T(4,128)(2,1)} %bitcast.15), calls=%async_computation.2 | async-start | bytes 16384 | tf_op jit(solution)/shard_map/all_to_all | solution.py:116
  14.7 15.2 %copy-start.14 = (s32[1,128,2]{1,2,0:T(2,128)S(1)}, s32[1,128,2]{1,2,0:T(2,128)}, u32[]{:S(2)}) copy-start(s32[1,128,2]{1,2,0:T(2,128)} %param.48) | copy-start | bytes 3076
  21.2 16.8 %all-to-all-start = ((bf16[128,8,256]{0,2,1:T(8,128)(2,1)}), bf16[128,8,256]{0,2,1:T(8,128)(2,1)S(1)}, u32[]{:S(2)}, u32[]{:S(2)}) async-start(bf16[128,8,256]{0,2,1:T(8,128)(2,1)} %bitcast.1), calls=%async_computation | async-start | bytes 1048576 | tf_op jit(solution)/shard_map/all_to_all | solution.py:114
  31.7 10.5 %copy-start.17 = (f32[4]{0:T(128)S(1)}, f32[4]{0:T(128)}, u32[]{:S(2)}) copy-start(f32[4]{0:T(128)} %dynamic_slice.29) | copy-start | bytes 52
  38.0 4.3 %copy-start.6 = (bf16[128,8,256]{0,2,1:T(8,128)(2,1)}, bf16[128,8,256]{0,2,1:T(8,128)(2,1)S(1)}, u32[]{:S(2)}) copy-start(bf16[128,8,256]{0,2,1:T(8,128)(2,1)S(1)} %all-to-all-done) | copy-start | bytes 1572868
  38.0 32.1 %all-to-all-start.1 = ((bf16[128,8,256]{2,0,1:T(8,128)(2,1)}), bf16[128,8,256]{2,0,1:T(8,128)(2,1)}, u32[]{:S(2)}, u32[]{:S(2)}) async-start(bf16[128,8,256]{2,0,1:T(8,128)(2,1)} %bitcast.7), calls=%async_computation.1 | async-start | bytes 1048576 | tf_op jit(solution)/shard_map/all_to_all | solution.py:115
  72.5 1.4 copy-start.1
  75.3 1.9 copy-start.2
  77.3 3.3 %copy-start.3 = (f32[1024,128]{1,0:T(8,128)}, f32[1024,128]{1,0:T(8,128)S(1)}, u32[]{:S(2)}) copy-start(f32[1024,128]{1,0:T(8,128)S(1)} %get-tuple-element.87) | copy-start | bytes 1572868
  102.0 9.5 %copy-start.13 = (f32[256]{0:T(256)S(1)}, f32[256]{0:T(256)}, u32[]{:S(2)}) copy-start(f32[256]{0:T(256)} %mul.258) | copy-start | bytes 3076
  111.5 8.2 %copy-start.8 = (s32[1,128,2]{2,1,0:T(8,128)S(1)}, s32[1,128,2]{2,1,0:T(8,128)}, u32[]{:S(2)}) copy-start(s32[1,128,2]{2,1,0:T(8,128)} %copy-done.7) | copy-start | bytes 3076
  113.7 9.6 %copy-start.15 = (s32[1,128,2]{1,2,0:T(2,128)S(1)}, s32[1,128,2]{1,2,0:T(2,128)}, u32[]{:S(2)}) copy-start(s32[1,128,2]{1,2,0:T(2,128)} %param.48) | copy-start | bytes 3076
  113.7 18.8 %all-to-all-start.3 = ((bf16[8,128,256]{2,1,0:T(8,128)(2,1)}), bf16[8,128,256]{2,1,0:T(8,128)(2,1)S(1)}, u32[]{:S(2)}, u32[]{:S(2)}) async-start(bf16[8,128,256]{2,1,0:T(8,128)(2,1)} %add_convert_fusion), calls=%async_computation.3 | async-start | bytes 1048576 | tf_op jit(solution)/shard_map/all_to_all | solution.py:145
  133.7 4.3 %copy-start.11 = (f32[2048]{0:T(1024)S(1)}, f32[2048]{0:T(1024)}, u32[]{:S(2)}) copy-start(f32[2048]{0:T(1024)} %param.39) | copy-start | bytes 24580
  136.2 1.8 copy-start.4
  139.2 5.0 %copy-start.12 = (f32[2048]{0:T(1024)S(1)}, f32[2048]{0:T(1024)}, u32[]{:S(2)}) copy-start(f32[2048]{0:T(1024)} %param.41) | copy-start | bytes 24580
  152.3 53.7 %copy-start.18 = (bf16[1,2048,512]{2,1,0:T(8,128)(2,1)S(1)}, bf16[1,2048,512]{2,1,0:T(8,128)(2,1)}, u32[]{:S(2)}) copy-start(bf16[1,2048,512]{2,1,0:T(8,128)(2,1)} %param.45) | copy-start | bytes 6291460
  204.7 1.3 copy-start.5
  214.5 3.8 %copy-start.16 = (f32[1,128,2]{1,2,0:T(2,128)S(1)}, f32[1,128,2]{1,2,0:T(2,128)}, u32[]{:S(2)}) copy-start(f32[1,128,2]{1,2,0:T(2,128)} %param.49) | copy-start | bytes 3076
  214.5 52.5 %all-to-all-start.5 = ((bf16[32,16,2048]{2,1,0:T(8,128)(2,1)}), bf16[32,16,2048]{2,1,0:T(8,128)(2,1)}, u32[]{:S(2)}, u32[]{:S(2)}) async-start(bf16[32,16,2048]{2,1,0:T(8,128)(2,1)} %convolution_convert_fusion), calls=%async_computation.5 | async-start | bytes 4194304 | tf_op jit(solution)/shard_map/all_to_all | solution.py:188
  (1 other events, 0.6 us)
Sparse Core Ops, SparseCore 0:
  8.9 60.9 all-gather.1
where the time goes:
time: 294 us; the launch traced here: 292 us
  waiting for transfers between devices  64.1 us (22%)
  other arithmetic  55.4 us (19%)
  blocking collectives  52.4 us (18%)
  local copies, waits for them, and re-layouts  43.4 us (15%)
  matrix products  38 us (13%)
  starting transfers between devices  24.9 us (8%)
  between operations  13.8 us (5%)
    all_to_all x1, blocking collectives, body(): lax.all_to_all(outgoing, ('sp', 'dp'), split_axis=0, concat_axis=0, tiled...  52.4 us
    all_to_all x1, waiting for transfers between devices, body(): lax.all_to_all(done, ('sp', 'dp'), split_axis=0, concat_axis=0, tiled=True)  46.4 us
    another operation x1, other arithmetic, block_scan(): cum = jnp.cumsum(logs, axis=1)  23.3 us
    unnamed x45, local copies, waits for them, and re-layouts  8.94 us
    all_to_all x1, waiting for transfers between devices, body(): lax.all_to_all(y, 'sp', split_axis=0, concat_axis=2, tiled=True)  8.85 us
    add x8, other arithmetic, advance(): return (carry * factor[:, None, None] + fresh, carry)  7.87 us
    all_to_all x1, starting transfers between devices, body(): lax.all_to_all(outgoing[2], 'sp', split_axis=1, concat_axis=0, tiled=True)  7.45 us
    scatter x1, local copies, waits for them, and re-layouts, body(): jnp.zeros((experts * slots, D), jnp.bfloat16).at[target]  7.19 us
  transfers between devices with their start and end apart: 6, of which 4 were waited for; matrix products, arithmetic and copies ran while one was open for 32% of the time, Pallas kernels for 0%

commit v1 on v0

v1 whole, which is shorter than its diff:
```python
import jax
import jax.numpy as jnp
from jax import lax
from jax.experimental import pallas as pl
from jax.experimental.pallas import tpu as pltpu
from jax.sharding import PartitionSpec as P

EPS = 1e-06
HIGH = lax.Precision.HIGHEST
HALO = 8
F32 = jnp.float32
BF16 = jnp.bfloat16


def silu(v):
    return v * (1.0 / (1.0 + jnp.exp(-v)))


def conv_silu(halo, rows, taps):
    count = taps.shape[0]
    length = rows.shape[0]
    padded = jnp.concatenate([halo.astype(F32), rows.astype(F32)], axis=0)
    total = None
    for tap in range(count):
        start = HALO - (count - 1) + tap
        term = padded[start : start + length] * taps[tap : tap + 1].astype(F32)
        total = term if total is None else total + term
    return silu(total)


def spread(columns, first, count, width):
    rows = columns.shape[0]
    return jnp.concatenate(
        [jnp.broadcast_to(columns[:, first + j : first + j + 1], (rows, width)) for j in range(count)],
        axis=1,
    )


def block_kernel(
    x_ref, b_ref, c_ref, halo_ref, step_ref, wx_ref, wb_ref, wc_ref, bias_ref, log_ref, skip_ref,
    y_ref, cm_ref, grow_ref, state_ref, *, groups,
):
    length, inner = x_ref.shape
    heads = step_ref.shape[1]
    span = b_ref.shape[1]
    per = heads // groups
    width = inner // heads
    state = span // groups
    wide = per * width
    raw = step_ref[...].astype(F32) + bias_ref[...]
    step = jnp.maximum(raw, 0.0) + jnp.log(1.0 + jnp.exp(-jnp.abs(raw)))
    logs = step * -jnp.exp(log_ref[...])
    row = lax.broadcasted_iota(jnp.int32, (length, length), 0)
    col = lax.broadcasted_iota(jnp.int32, (length, length), 1)
    lower = row >= col
    tril = lower.astype(F32)
    cum = lax.dot_general(tril, logs, (((1,), (0,)), ((), ())), precision=HIGH, preferred_element_type=F32)
    cum_t = lax.dot_general(logs, tril, (((0,), (1,)), ((), ())), precision=HIGH, preferred_element_type=F32)
    grow_ref[...] = cum
    to_end = jnp.exp(cum[length - 1 : length] - cum)
    for g in range(groups):
        xcol = slice(g * wide, (g + 1) * wide)
        bcol = slice(g * state, (g + 1) * state)
        xs = conv_silu(halo_ref[:, xcol], x_ref[:, xcol], wx_ref[:, xcol])
        bm = conv_silu(
            halo_ref[:, inner + g * state : inner + (g + 1) * state], b_ref[:, bcol], wb_ref[:, bcol]
        ).astype(BF16)
        cm = conv_silu(
            halo_ref[:, inner + span + g * state : inner + span + (g + 1) * state],
            c_ref[:, bcol], wc_ref[:, bcol],
        ).astype(BF16)
        cm_ref[:, bcol] = cm
        weighted = xs * spread(step, g * per, per, width)
        scores = lax.dot_general(cm, bm, (((1,), (1,)), ((), ())), preferred_element_type=F32)
        scores = jnp.where(lower, scores, 0.0)
        parts = []
        small = weighted.astype(BF16)
        for j in range(per):
            h = g * per + j
            decay = jnp.exp(jnp.minimum(cum[:, h : h + 1] - cum_t[h : h + 1, :], 0.0))
            parts.append(
                jnp.dot((scores * decay).astype(BF16), small[:, j * width : (j + 1) * width],
                        preferred_element_type=F32)
            )
        y_ref[:, xcol] = jnp.concatenate(parts, axis=1) + skip_ref[:, xcol] * xs
        ended = (weighted * spread(to_end, g * per, per, width)).astype(BF16)
        state_ref[xcol, :] = lax.dot_general(
            ended, bm, (((0,), (0,)), ((), ())), preferred_element_type=F32
        ).astype(BF16)


def norm_kernel(y_ref, cm_ref, grow_ref, before_ref, gate_ref, gain_ref, out_ref, *, groups):
    length, inner = y_ref.shape
    heads = grow_ref.shape[1]
    state = before_ref.shape[1]
    per = heads // groups
    width = inner // heads
    wide = per * width
    grow = jnp.exp(grow_ref[...])
    for g in range(groups):
        xcol = slice(g * wide, (g + 1) * wide)
        outer = lax.dot_general(
            cm_ref[:, g * state : (g + 1) * state], before_ref[xcol, :],
            (((1,), (1,)), ((), ())), preferred_element_type=F32,
        )
        v = y_ref[:, xcol] + outer * spread(grow, g * per, per, width)
        v = v * silu(gate_ref[:, xcol].astype(F32))
        v = v * lax.rsqrt(jnp.mean(v * v, axis=1, keepdims=True) + EPS)
        out_ref[:, xcol] = (v * gain_ref[:, xcol]).astype(BF16)


def vmem(count):
    return [pl.BlockSpec(memory_space=pltpu.VMEM)] * count


PARAMS = pltpu.CompilerParams(vmem_limit_bytes=32 * 1024 * 1024)


def body(
    residual, head_input, gate_input, b_input, c_input, step_input, conv_weight, conv_b_weight,
    conv_c_weight, step_bias, decay_log, skip, norm_gain, out_weight, ffn_gain, shared_gate,
    shared_up, shared_down, expert_gate, expert_up, expert_down, routes, route_weights,
):
    tokens, inner = head_input.shape[1:]
    heads = step_bias.shape[0]
    state = 128
    span = b_input.shape[2]
    groups = span // state
    width = inner // heads
    model = residual.shape[2]
    ways = lax.axis_size("sp")
    place = lax.axis_index("sp")
    local = heads // ways
    x_rows, b_rows, c_rows = head_input[0], b_input[0], c_input[0]
    weight = lax.all_gather(out_weight, "dp", axis=0, tiled=True)
    tail = jnp.concatenate([x_rows[-HALO:], b_rows[-HALO:], c_rows[-HALO:]], axis=1)
    halo = lax.ppermute(tail, "sp", [(i, i + 1) for i in range(ways - 1)])
    y, cm, cum, states = pl.pallas_call(
        lambda *refs: block_kernel(*refs, groups=groups),
        out_shape=(
            jax.ShapeDtypeStruct((tokens, inner), F32),
            jax.ShapeDtypeStruct((tokens, span), BF16),
            jax.ShapeDtypeStruct((tokens, heads), F32),
            jax.ShapeDtypeStruct((inner, state), BF16),
        ),
        in_specs=vmem(11),
        out_specs=tuple(vmem(4)),
        compiler_params=PARAMS,
        cost_estimate=pl.CostEstimate(flops=400_000_000, bytes_accessed=5_000_000, transcendentals=1_500_000),
    )(
        x_rows, b_rows, c_rows, halo, step_input[0], conv_weight, conv_b_weight, conv_c_weight,
        step_bias[None], decay_log[None], jnp.repeat(skip, width)[None],
    )
    totals = lax.all_gather(cum[-1:], "sp", axis=0, tiled=True)
    arrived = lax.all_to_all(
        states.reshape(ways, local * width, state), "sp", split_axis=0, concat_axis=0, tiled=True
    )
    factors = jnp.repeat(
        jnp.exp(lax.dynamic_slice_in_dim(totals, place * local, local, 1)), width, axis=1
    )[:, :, None]
    carry = jnp.zeros((local * width, state), F32)
    prefix = []
    for i in range(ways):
        prefix.append(carry.astype(BF16))
        carry = carry * factors[i] + arrived[i].astype(F32)
    before = lax.all_to_all(jnp.stack(prefix), "sp", split_axis=0, concat_axis=0, tiled=True).reshape(
        inner, state
    )
    normed = pl.pallas_call(
        lambda *refs: norm_kernel(*refs, groups=groups),
        out_shape=jax.ShapeDtypeStruct((tokens, inner), BF16),
        in_specs=vmem(6),
        out_specs=vmem(1)[0],
        compiler_params=PARAMS,
        cost_estimate=pl.CostEstimate(flops=100_000_000, bytes_accessed=3_000_000, transcendentals=400_000),
    )(y, cm, cum, before, gate_input[0], norm_gain[None])

    mixed = (residual[0].astype(F32) + jnp.dot(normed, weight, preferred_element_type=F32)).astype(BF16)
    mixed_f = mixed.astype(F32)
    expert_in = (
        mixed_f * lax.rsqrt(jnp.mean(mixed_f * mixed_f, axis=1, keepdims=True) + EPS) * ffn_gain[None, :]
    ).astype(BF16)

    picks = routes.shape[2]
    ranks = ways * lax.axis_size("dp")
    experts = ranks * expert_gate.shape[0]
    slots = 2 * tokens * picks // experts
    chosen = routes[0].reshape(-1)
    pairs = chosen.shape[0]
    onehot = (chosen[:, None] == jnp.arange(experts, dtype=jnp.int32)[None, :]).astype(BF16)
    earlier = (jnp.arange(pairs)[:, None] > jnp.arange(pairs)[None, :]).astype(BF16)
    counts = jnp.dot(earlier, onehot, preferred_element_type=F32)
    position = jnp.sum(counts * onehot.astype(F32), axis=1).astype(jnp.int32)
    target = (chosen * slots + position).reshape(tokens, picks)
    lanes = jnp.arange(experts * slots, dtype=jnp.int32)
    combine = jnp.zeros((tokens, experts * slots), F32)
    choose = jnp.zeros((experts * slots, tokens), BF16)
    for k in range(picks):
        combine = combine + jnp.where(target[:, k, None] == lanes[None, :], route_weights[0][:, k, None], 0.0)
        choose = choose + (lanes[:, None] == target[None, :, k]).astype(BF16)
    high = combine.astype(BF16)
    low = (combine - high.astype(F32)).astype(BF16)

    outgoing = jnp.dot(choose, expert_in, preferred_element_type=F32).astype(BF16)
    got = lax.all_to_all(
        outgoing.reshape(experts, slots, model), ("sp", "dp"), split_axis=0, concat_axis=0, tiled=True
    )
    own = expert_gate.shape[0]
    shaped = got.reshape(ranks, own, slots, model)
    if own == 1:
        flat = got.reshape(ranks * slots, model)
        gate = jnp.dot(flat, expert_gate[0], preferred_element_type=F32)
        up = jnp.dot(flat, expert_up[0], preferred_element_type=F32)
        hidden = (jax.nn.silu(gate) * up).astype(BF16)
        done = jnp.dot(hidden, expert_down[0], preferred_element_type=F32).astype(BF16)
    else:
        gate = jnp.einsum("aenc,ecf->aenf", shaped, expert_gate, preferred_element_type=F32)
        up = jnp.einsum("aenc,ecf->aenf", shaped, expert_up, preferred_element_type=F32)
        hidden = (jax.nn.silu(gate) * up).astype(BF16)
        done = jnp.einsum("aenf,efc->aenc", hidden, expert_down, preferred_element_type=F32).astype(BF16)
    returned = lax.all_to_all(
        done.reshape(experts, slots, model), ("sp", "dp"), split_axis=0, concat_axis=0, tiled=True
    ).reshape(experts * slots, model)
    shared_hidden = (
        jax.nn.silu(jnp.dot(expert_in, shared_gate, preferred_element_type=F32))
        * jnp.dot(expert_in, shared_up, preferred_element_type=F32)
    ).astype(BF16)
    shared = mixed_f + jnp.dot(shared_hidden, shared_down, preferred_element_type=F32)
    routed = jnp.dot(high, returned, preferred_element_type=F32) + jnp.dot(
        low, returned, preferred_element_type=F32
    )
    return (shared + routed).astype(BF16)[None]


def solution(mesh):
    rows = P("dp", "sp", None)
    split = P(("sp", "dp"), None, None)
    return jax.shard_map(
        body,
        mesh=mesh,
        in_specs=(rows,) * 6 + (P(),) * 7 + (P("dp", None),) + (P(),) * 4 + (split,) * 3 + (rows,) * 2,
        out_specs=rows,
        check_vma=False,
    )
```

time: 294 us -> 209 us (0.71)
  other arithmetic: 55.4 us -> 5.49 us
  local copies, waits for them, and re-layouts: 43.4 us -> 9.36 us
  blocking collectives: 52.4 us -> 73.6 us
  matrix products: 38 us -> 24.3 us
  waiting for transfers between devices: 64.1 us -> 55.8 us
  Pallas kernels: 0 us -> 7.14 us
  starting transfers between devices: 24.9 us -> 19 us
    another operation x3 -> x1, other arithmetic: 23.9 us -> 0.75 us  [body(): jnp.stack(prefix)]
    all_gather x0 -> x1, blocking collectives: none -> 21.4 us  [body(): totals = lax.all_gather(cum[-1:], 'sp', axis=0, tiled=True)]
    dot_general x9, matrix products: 38 us -> 24.3 us  [the longest x1 5.98 us: body(): jnp.dot(hidden, expert_down[0], preferred_element_type=F32).astype(BF16)]
    all_to_all x5 -> x3, starting transfers between devices: 24.9 us -> 14.1 us  [the longest x1 6.81 us: body(): lax.all_to_all(states.reshape(ways, local * width, state), 'sp', split_ax...]
    all_to_all x5 -> x3, waiting for transfers between devices: 63.4 us -> 53.5 us  [the longest x1 42.5 us: body(): lax.all_to_all(done.reshape(experts, slots, model), ('sp', 'dp'), split_a...]
    add x8 -> x1, other arithmetic: 7.87 us -> 0.01 us  [body(): target = (chosen * slots + position).reshape(tokens, picks)]
    reduce_sum x3 -> x0, other arithmetic: 7.56 us -> none  [the longest x1 5.71 us: body(): jnp.sum(pair_out.reshape(tokens, TOP_K, D).astype(jnp.float32) * route_we...]
    scatter x1 -> x0, local copies, waits for them, and re-layouts: 7.19 us -> none  [body(): jnp.zeros((experts * slots, D), jnp.bfloat16).at[target]]
  transfers between devices with their start and end apart: 6 -> 5, of which waited for: 4 -> 3; matrix products, arithmetic and copies ran while one was open for 32% -> 7% of each run, Pallas kernels for 0% -> 3%
where the time goes in v1:
time: 209 us; the launch traced here: 208 us
  blocking collectives  73.6 us (35%)
  waiting for transfers between devices  55.8 us (27%)
  matrix products  24.3 us (12%)
  starting transfers between devices  19 us (9%)
  between operations  13.7 us (7%)
  local copies, waits for them, and re-layouts  9.36 us (4%)
  Pallas kernels  7.14 us (3%)
  other arithmetic  5.49 us (3%)
    all_to_all x1, blocking collectives, body(): lax.all_to_all(outgoing.reshape(experts, slots, model), ('sp', 'dp'), spl...  52.2 us
    all_to_all x1, waiting for transfers between devices, body(): lax.all_to_all(done.reshape(experts, slots, model), ('sp', 'dp'), split_a...  42.5 us
    all_gather x1, blocking collectives, body(): totals = lax.all_gather(cum[-1:], 'sp', axis=0, tiled=True)  21.4 us
    all_to_all x1, waiting for transfers between devices, body(): lax.all_to_all(jnp.stack(prefix), 'sp', split_axis=0, concat_axis=0, tile...  11 us
    unnamed x50, local copies, waits for them, and re-layouts  6.88 us
    all_to_all x1, starting transfers between devices, body(): lax.all_to_all(states.reshape(ways, local * width, state), 'sp', split_ax...  6.81 us
    dot_general x1, matrix products, body(): jnp.dot(hidden, expert_down[0], preferred_element_type=F32).astype(BF16)  5.98 us
    pallas_call x1, Pallas kernels, body(): pl.pallas_call(lambda *refs: block_kernel(*refs, groups=groups), out_shap...  5.65 us
  transfers between devices with their start and end apart: 5, of which 3 were waited for; matrix products, arithmetic and copies ran while one was open for 7% of the time, Pallas kernels for 3%

profile of v1, /device:TPU:0, one launch (start us, length us, event | category | flops | bytes accessed | tf_op | source)
XLA Modules:
  0.0 208.5 jit_solution(5172249626928963992)
XLA Ops:
  8.4 4.9 %collective-permute-start = (bf16[8,4096]{1,0:T(8,128)(2,1)S(1)}, bf16[8,4096]{1,0:T(8,128)(2,1)S(1)}, u32[]{:S(2)}, u32[]{:S(2)}) collective-permute-start(bf16[8,4096]{1,0:T(8,128)(2,1)S(1)} %pad_maximum_fusion), channel_id=1, source_target_pairs={{0,4},{4,8},{8,12},{12,16},{16,20},{20,24},{24,28},{1,5},{5,9},{9,... | collective-permute-start | bytes 196616 | tf_op jit(solution)/shard_map/ppermute | solution.py:137
  13.6 1.6 collective-permute-done.refs_3_
  15.2 0.9 copy-done.7
  16.2 5.6 %shard_map.217 = (f32[128,2048]{1,0:T(8,128)S(1)}, bf16[128,1024]{1,0:T(8,128)(2,1)S(1)}, f32[128,32]{1,0:T(8,128)S(1)}, bf16[2048,128]{1,0:T(8,128)(2,1)}) custom-call(bf16[128,2048]{1,0:T(8,128)(2,1)S(1)} %bitcast.76, bf16[128,1024]{1,0:T(8,128)(2,1)S(1)} %bitcast.77, bf16[128,1024]{1,0:T(8,128)(2,1)S(1)} %bitcast.78, ...), custom_call_target="tpu_custom_call" | custom-call | flops 400000000 | bytes 5000000 | tf_op jit(solution)/shard_map/pallas_call | solution.py:138
  21.8 1.1 copy-done.1
  22.9 6.8 %all-to-all-start = ((bf16[8,256,128]{2,1,0:T(8,128)(2,1)}), bf16[8,256,128]{2,1,0:T(8,128)(2,1)S(1)}, u32[]{:S(2)}, u32[]{:S(2)}) async-start(bf16[8,256,128]{2,1,0:T(8,128)(2,1)} %bitcast.12), calls=%async_computation | async-start | bytes 1048576 | tf_op jit(solution)/shard_map/all_to_all | solution.py:155
  30.3 21.4 %all-gather = f32[8,1,32]{2,1,0:T(1,128)S(1)} all-gather(f32[1,1,32]{2,1,0:T(1,128)S(1)} %slice_bitcast_fusion.11), channel_id=1, replica_groups=mesh['sp'=8,'dp'=4] {'sp'}, dimensions={0}, use_global_device_ids=true | all-gather | bytes 1152 | tf_op jit(solution)/shard_map/all_gather | solution.py:154
  56.0 0.9 convert_dynamic-update-slice_fusion
  58.4 3.5 %all-to-all-start.1 = ((bf16[8,256,128]{2,1,0:T(8,128)(2,1)}), bf16[8,256,128]{2,1,0:T(8,128)(2,1)S(1)}, u32[]{:S(2)}, u32[]{:S(2)}) async-start(bf16[8,256,128]{2,1,0:T(8,128)(2,1)} %fusion.51), calls=%async_computation.1 | async-start | bytes 1048576 | tf_op jit(solution)/shard_map/all_to_all | solution.py:166
  62.7 11.0 %all-to-all-done.1 = bf16[8,256,128]{2,1,0:T(8,128)(2,1)S(1)} async-done(((bf16[8,256,128]{2,1,0:T(8,128)(2,1)}), bf16[8,256,128]{2,1,0:T(8,128)(2,1)S(1)}, u32[]{:S(2)}, u32[]{:S(2)}) %all-to-all-start.1) | async-done | bytes 524320 | tf_op jit(solution)/shard_map/all_to_all | solution.py:166
  73.7 1.2 copy-done.2
  75.0 1.0 copy-done.3
  76.0 1.5 shard_map.218
  77.5 4.9 %multiply_reduce_fusion = (f32[128]{0:T(128)S(1)}, f32[128,2048]{1,0:T(8,128)S(1)}) fusion(bf16[128,2048]{1,0:T(8,128)(2,1)S(1)} %shard_map.218, bf16[2048,2048]{1,0:T(8,128)(2,1)} %all-gather.3.cloned.1.call-done, bf16[1,128,2048]{2,1,0:T(8,128)(2,1)} %param.23), kind=kOutput, calls=%fused_computation.22 | convolution fusion | flops 1075314560 | bytes 10486272 | tf_op jit(solution)/shard_map/dot_general | solution.py:178
  83.2 52.2 %all_to_all.20 = bf16[32,16,2048]{2,1,0:T(8,128)(2,1)S(1)} all-to-all(bf16[32,16,2048]{2,1,0:T(8,128)(2,1)S(1)} %bitcast.81), channel_id=1, replica_groups=mesh['sp'=8,'dp'=4] {'sp','dp'}, dimensions={0} | all-to-all | bytes 4194304 | tf_op jit(solution)/shard_map/all_to_all | solution.py:205
  135.4 1.3 copy-done.16
  136.8 1.3 fusion.8
  138.0 6.0 %convolution_convert_fusion.1 = bf16[512,2048]{1,0:T(8,128)(2,1)} fusion(bf16[1,512,2048]{2,1,0:T(8,128)(2,1)S(1)} %copy-done, bf16[512,2048]{1,0:T(8,128)(2,1)} %bitcast.84, bf16[1,2048,512]{2,1,0:T(8,128)(2,1)} %param.42, f32[512,512]{1,0:T(8,128)S(1)} %fusion.8), kind=kOutput, calls=%fused_computation.1 | convolution fusion | flops 2150105088 | bytes 9437184 | tf_op jit(solution)/shard_map/dot_general | solution.py:215
  144.0 3.8 %all-to-all-start.3 = ((bf16[32,16,2048]{2,1,0:T(8,128)(2,1)}), bf16[32,16,2048]{2,1,0:T(8,128)(2,1)}, u32[]{:S(2)}, u32[]{:S(2)}) async-start(bf16[32,16,2048]{2,1,0:T(8,128)(2,1)} %bitcast.82), calls=%async_computation.3 | async-start | bytes 4194304 | tf_op jit(solution)/shard_map/all_to_all | solution.py:221
  147.9 2.1 fusion.59
  149.9 4.1 %convolution_add_fusion.1 = f32[128,2048]{1,0:T(8,128)} fusion(f32[128,2048]{1,0:T(8,128)S(1)} %copy-done.14, bf16[512,2048]{1,0:T(8,128)(2,1)} %param.40, bf16[2048,512]{1,0:T(8,128)(2,1)} %param.39, f32[128,512]{1,0:T(8,128)S(1)} %fusion.59, f32[2048]{0:T(1024)S(1)} %copy-done.17, f32[128]{0:T(128)S(1)} %add_rsqrt_fusion), kind=kOutput, calls=%fused_computation.4 | convolution fusion | flops 538312704 | bytes 6562304 | tf_op jit(solution)/shard_map/dot_general | solution.py:228
  154.0 42.5 %all-to-all-done.3 = bf16[32,16,2048]{2,1,0:T(8,128)(2,1)} async-done(((bf16[32,16,2048]{2,1,0:T(8,128)(2,1)}), bf16[32,16,2048]{2,1,0:T(8,128)(2,1)}, u32[]{:S(2)}, u32[]{:S(2)}) %all-to-all-start.3) | async-done | bytes 2097184 | tf_op jit(solution)/shard_map/all_to_all | solution.py:221
  196.5 2.1 %fusion.42 = f32[128,2048]{1,0:T(8,128)S(1)} fusion(bf16[512,2048]{1,0:T(8,128)(2,1)} %bitcast.32, f32[128]{0:T(128)S(1)} %get-tuple-element.25, s32[128]{0:T(128)S(1)} %get-tuple-element.14, f32[128]{0:T(128)S(1)} %get-tuple-element.24, s32[128]{0:T(128)S(1)} %get-tuple-element.13), kind=kOutput, calls=%fused_computation.56 | convolution fusion | flops 268828672 | bytes 3147776 | tf_op jit(solution)/shard_map/dot_general | solution.py:229
  198.7 3.0 %fusion.4 = bf16[1,128,2048]{2,1,0:T(8,128)(2,1)} fusion(f32[128,2048]{1,0:T(8,128)S(1)} %copy-done.15, f32[128,2048]{1,0:T(8,128)S(1)} %fusion.42, bf16[512,2048]{1,0:T(8,128)(2,1)} %bitcast.32, f32[128]{0:T(128)S(1)} %get-tuple-element.25, s32[128]{0:T(128)S(1)} %get-tuple-element.14, f32[128]{0:T(128)S(1)} %get-tuple-element.24, s32[128]{0:T(128)S(1)} %get-tuple-element.13), kind=kOutput, calls=%fused_computation.9 | convolution fusion | flops 269811712 | bytes 4720640 | tf_op jit(solution)/shard_map/dot_general | solution.py:229
  (85 shorter events, 10.1 us)
Async XLA Ops:
  6.5 131.5 %copy-start = (bf16[1,512,2048]{2,1,0:T(8,128)(2,1)S(1)}, bf16[1,512,2048]{2,1,0:T(8,128)(2,1)}, u32[]{:S(2)}) copy-start(bf16[1,512,2048]{2,1,0:T(8,128)(2,1)} %param.43) | copy-start | bytes 6291460
  6.5 1.8 copy-start.5
  6.5 6.8 %copy-start.18 = (bf16[1,128,32]{1,2,0:T(8,128)(2,1)S(1)}, bf16[1,128,32]{1,2,0:T(8,128)(2,1)}, u32[]{:S(2)}) copy-start(bf16[1,128,32]{1,2,0:T(8,128)(2,1)} %param.28) | copy-start | bytes 24580
  6.5 6.9 %copy-start.21 = (f32[32]{0:T(128)S(1)}, f32[32]{0:T(128)}, u32[]{:S(2)}) copy-start(f32[32]{0:T(128)} %param.34) | copy-start | bytes 388
  6.5 8.6 %copy-start.11 = (f32[32]{0:T(128)S(1)}, f32[32]{0:T(128)}, u32[]{:S(2)}) copy-start(f32[32]{0:T(128)} %param.32) | copy-start | bytes 388
  6.6 8.6 %copy-start.12 = (f32[32]{0:T(128)S(1)}, f32[32]{0:T(128)}, u32[]{:S(2)}) copy-start(f32[32]{0:T(128)} %param.33) | copy-start | bytes 388
  6.6 8.6 %copy-start.8 = (bf16[4,2048]{1,0:T(4,128)(2,1)S(1)}, bf16[4,2048]{1,0:T(4,128)(2,1)}, u32[]{:S(2)}) copy-start(bf16[4,2048]{1,0:T(4,128)(2,1)} %refs_5_.1) | copy-start | bytes 49156
  6.6 8.6 %copy-start.9 = (bf16[4,1024]{1,0:T(4,128)(2,1)S(1)}, bf16[4,1024]{1,0:T(4,128)(2,1)}, u32[]{:S(2)}) copy-start(bf16[4,1024]{1,0:T(4,128)(2,1)} %refs_6_.1) | copy-start | bytes 24580
  6.6 8.6 %copy-start.10 = (bf16[4,1024]{1,0:T(4,128)(2,1)S(1)}, bf16[4,1024]{1,0:T(4,128)(2,1)}, u32[]{:S(2)}) copy-start(bf16[4,1024]{1,0:T(4,128)(2,1)} %refs_7_.1) | copy-start | bytes 24580
  6.6 70.9 %all-gather.3.cloned.1.call-start = ((), (), s32[]{:S(2)}) async-start(), calls=%async_computation.4 | async-start | bytes 10485760 | tf_op jit(solution)/shard_map/all_gather | solution.py:135
  8.4 6.8 %collective-permute-start = (bf16[8,4096]{1,0:T(8,128)(2,1)S(1)}, bf16[8,4096]{1,0:T(8,128)(2,1)S(1)}, u32[]{:S(2)}, u32[]{:S(2)}) collective-permute-start(bf16[8,4096]{1,0:T(8,128)(2,1)S(1)} %pad_maximum_fusion), channel_id=1, source_target_pairs={{0,4},{4,8},{8,12},{12,16},{16,20},{20,24},{24,28},{1,5},{5,9},{9,... | collective-permute-start | bytes 196616 | tf_op jit(solution)/shard_map/ppermute | solution.py:137
  22.9 39.0 %copy-start.19 = (s32[1,128,2]{1,2,0:T(2,128)S(1)}, s32[1,128,2]{1,2,0:T(2,128)}, u32[]{:S(2)}) copy-start(s32[1,128,2]{1,2,0:T(2,128)} %param.44) | copy-start | bytes 3076
  22.9 30.1 %all-to-all-start = ((bf16[8,256,128]{2,1,0:T(8,128)(2,1)}), bf16[8,256,128]{2,1,0:T(8,128)(2,1)S(1)}, u32[]{:S(2)}, u32[]{:S(2)}) async-start(bf16[8,256,128]{2,1,0:T(8,128)(2,1)} %bitcast.12), calls=%async_computation | async-start | bytes 1048576 | tf_op jit(solution)/shard_map/all_to_all | solution.py:155
  29.7 44.1 %copy-start.4 = (f32[2048]{0:T(1024)S(1)}, f32[2048]{0:T(1024)}, u32[]{:S(2)}) copy-start(f32[2048]{0:T(1024)} %param.35) | copy-start | bytes 24580
  58.4 15.3 %all-to-all-start.1 = ((bf16[8,256,128]{2,1,0:T(8,128)(2,1)}), bf16[8,256,128]{2,1,0:T(8,128)(2,1)S(1)}, u32[]{:S(2)}, u32[]{:S(2)}) async-start(bf16[8,256,128]{2,1,0:T(8,128)(2,1)} %fusion.51), calls=%async_computation.1 | async-start | bytes 1048576 | tf_op jit(solution)/shard_map/all_to_all | solution.py:166
  73.7 1.2 copy-start.2
  77.5 4.9 %copy-start.17 = (f32[2048]{0:T(1024)S(1)}, f32[2048]{0:T(1024)}, u32[]{:S(2)}) copy-start(f32[2048]{0:T(1024)} %param.37) | copy-start | bytes 24580
  82.4 53.0 %copy-start.13 = (f32[128,2048]{1,0:T(8,128)}, f32[128,2048]{1,0:T(8,128)S(1)}, u32[]{:S(2)}) copy-start(f32[128,2048]{1,0:T(8,128)S(1)} %get-tuple-element.27) | copy-start | bytes 3145732
  83.2 53.5 %copy-start.22 = (bf16[1,2048,512]{2,1,0:T(8,128)(2,1)S(1)}, bf16[1,2048,512]{2,1,0:T(8,128)(2,1)}, u32[]{:S(2)}) copy-start(bf16[1,2048,512]{2,1,0:T(8,128)(2,1)} %param.41) | copy-start | bytes 6291460
  135.4 1.3 copy-start.16
  144.0 3.8 %copy-start.20 = (f32[1,128,2]{1,2,0:T(2,128)S(1)}, f32[1,128,2]{1,2,0:T(2,128)}, u32[]{:S(2)}) copy-start(f32[1,128,2]{1,2,0:T(2,128)} %param.45) | copy-start | bytes 3076
  144.0 3.8 %copy-start.14 = (f32[128,2048]{1,0:T(8,128)S(1)}, f32[128,2048]{1,0:T(8,128)}, u32[]{:S(2)}) copy-start(f32[128,2048]{1,0:T(8,128)} %copy-done.13) | copy-start | bytes 3145732
  144.0 52.5 %all-to-all-start.3 = ((bf16[32,16,2048]{2,1,0:T(8,128)(2,1)}), bf16[32,16,2048]{2,1,0:T(8,128)(2,1)}, u32[]{:S(2)}, u32[]{:S(2)}) async-start(bf16[32,16,2048]{2,1,0:T(8,128)(2,1)} %bitcast.82), calls=%async_computation.3 | async-start | bytes 4194304 | tf_op jit(solution)/shard_map/all_to_all | solution.py:221
  154.0 44.6 %copy-start.15 = (f32[128,2048]{1,0:T(8,128)S(1)}, f32[128,2048]{1,0:T(8,128)}, u32[]{:S(2)}) copy-start(f32[128,2048]{1,0:T(8,128)} %convolution_add_fusion.1) | copy-start | bytes 3145732
  (4 other events, 4.2 us)
Sparse Core Ops, SparseCore 0:
  9.0 60.9 all-gather.2

commit v2 on v1

--- a/solution.py
+++ b/solution.py
@@ -8,6 +8,7 @@
 EPS = 1e-06
 HIGH = lax.Precision.HIGHEST
 HALO = 8
+TAIL = 16
 F32 = jnp.float32
 BF16 = jnp.bfloat16
 
@@ -38,7 +39,7 @@
 
 def block_kernel(
     x_ref, b_ref, c_ref, halo_ref, step_ref, wx_ref, wb_ref, wc_ref, bias_ref, log_ref, skip_ref,
-    y_ref, cm_ref, grow_ref, state_ref, *, groups,
+    y_ref, cm_ref, grow_ref, state_ref, *, groups, local,
 ):
     length, inner = x_ref.shape
     heads = step_ref.shape[1]
@@ -84,9 +85,41 @@
             )
         y_ref[:, xcol] = jnp.concatenate(parts, axis=1) + skip_ref[:, xcol] * xs
         ended = (weighted * spread(to_end, g * per, per, width)).astype(BF16)
-        state_ref[xcol, :] = lax.dot_general(
+        fresh = lax.dot_general(
             ended, bm, (((0,), (0,)), ((), ())), preferred_element_type=F32
         ).astype(BF16)
+        for j in range(per):
+            h = g * per + j
+            at = h % local * width
+            state_ref[h // local, at : at + width, :] = fresh[j * width : (j + 1) * width]
+    last = cum[length - 1 : length]
+    high = last.astype(BF16)
+    rest = last - high.astype(F32)
+    middle = rest.astype(BF16)
+    low = (rest - middle.astype(F32)).astype(BF16)
+    for w in range(heads // local):
+        mine = slice(w * local, (w + 1) * local)
+        parts = [p.astype(F32)[:, mine] for p in (high, middle, low)]
+        rows = jnp.concatenate(parts + [jnp.zeros((TAIL - 3, local), F32)], axis=0)
+        rows = jnp.concatenate([rows, jnp.zeros((TAIL, state - local), F32)], axis=1)
+        state_ref[w, local * width :, :] = rows.astype(BF16)
+
+
+def prefix_kernel(got_ref, out_ref, *, local):
+    ways, rows, state = out_ref.shape
+    width = rows // local
+    factors = []
+    for i in range(ways - 1):
+        tail = got_ref[i, rows : rows + TAIL, :].astype(F32)
+        factors.append(jnp.exp(tail[0:1] + tail[1:2] + tail[2:3]))
+    for j in range(local):
+        at = slice(j * width, (j + 1) * width)
+        carry = jnp.zeros((width, state), F32)
+        for i in range(ways):
+            out_ref[i, at, :] = carry.astype(BF16)
+            if i < ways - 1:
+                factor = jnp.broadcast_to(factors[i][:, j : j + 1], (1, state))
+                carry = carry * factor + got_ref[i, at, :].astype(F32)
 
 
 def norm_kernel(y_ref, cm_ref, grow_ref, before_ref, gate_ref, gain_ref, out_ref, *, groups):
@@ -129,19 +162,18 @@
     width = inner // heads
     model = residual.shape[2]
     ways = lax.axis_size("sp")
-    place = lax.axis_index("sp")
     local = heads // ways
     x_rows, b_rows, c_rows = head_input[0], b_input[0], c_input[0]
     weight = lax.all_gather(out_weight, "dp", axis=0, tiled=True)
     tail = jnp.concatenate([x_rows[-HALO:], b_rows[-HALO:], c_rows[-HALO:]], axis=1)
     halo = lax.ppermute(tail, "sp", [(i, i + 1) for i in range(ways - 1)])
     y, cm, cum, states = pl.pallas_call(
-        lambda *refs: block_kernel(*refs, groups=groups),
+        lambda *refs: block_kernel(*refs, groups=groups, local=local),
         out_shape=(
             jax.ShapeDtypeStruct((tokens, inner), F32),
             jax.ShapeDtypeStruct((tokens, span), BF16),
             jax.ShapeDtypeStruct((tokens, heads), F32),
-            jax.ShapeDtypeStruct((inner, state), BF16),
+            jax.ShapeDtypeStruct((ways, local * width + TAIL, state), BF16),
         ),
         in_specs=vmem(11),
         out_specs=tuple(vmem(4)),
@@ -151,21 +183,16 @@
         x_rows, b_rows, c_rows, halo, step_input[0], conv_weight, conv_b_weight, conv_c_weight,
         step_bias[None], decay_log[None], jnp.repeat(skip, width)[None],
     )
-    totals = lax.all_gather(cum[-1:], "sp", axis=0, tiled=True)
-    arrived = lax.all_to_all(
-        states.reshape(ways, local * width, state), "sp", split_axis=0, concat_axis=0, tiled=True
-    )
-    factors = jnp.repeat(
-        jnp.exp(lax.dynamic_slice_in_dim(totals, place * local, local, 1)), width, axis=1
-    )[:, :, None]
-    carry = jnp.zeros((local * width, state), F32)
-    prefix = []
-    for i in range(ways):
-        prefix.append(carry.astype(BF16))
-        carry = carry * factors[i] + arrived[i].astype(F32)
-    before = lax.all_to_all(jnp.stack(prefix), "sp", split_axis=0, concat_axis=0, tiled=True).reshape(
-        inner, state
-    )
+    arrived = lax.all_to_all(states, "sp", split_axis=0, concat_axis=0, tiled=True)
+    prefix = pl.pallas_call(
+        lambda *refs: prefix_kernel(*refs, local=local),
+        out_shape=jax.ShapeDtypeStruct((ways, local * width, state), BF16),
+        in_specs=vmem(1),
+        out_specs=vmem(1)[0],
+        compiler_params=PARAMS,
+        cost_estimate=pl.CostEstimate(flops=2_000_000, bytes_accessed=1_000_000, transcendentals=1000),
+    )(arrived)
+    before = lax.all_to_all(prefix, "sp", split_axis=0, concat_axis=0, tiled=True).reshape(inner, state)
     normed = pl.pallas_call(
         lambda *refs: norm_kernel(*refs, groups=groups),
         out_shape=jax.ShapeDtypeStruct((tokens, inner), BF16),

time: 209 us -> 203 us (0.971)
  starting transfers between devices: 19 us -> 12.2 us
  waiting for transfers between devices: 55.8 us -> 62.2 us
  other arithmetic: 5.49 us -> 0.03 us
  local copies, waits for them, and re-layouts: 9.36 us -> 6.2 us
    all_gather x1 -> x0, blocking collectives: 21.4 us -> none  [body(): totals = lax.all_gather(cum[-1:], 'sp', axis=0, tiled=True)]
    all_to_all x0 -> x1, blocking collectives: none -> 21.4 us  [body(): lax.all_to_all(states, 'sp', split_axis=0, concat_axis=0, tiled=True)]
    all_to_all x2 -> x1, starting transfers between devices: 10.3 us -> 3.49 us  [body(): lax.all_to_all(prefix, 'sp', split_axis=0, concat_axis=0, tiled=True)]
    all_gather x1, waiting for transfers between devices: 0.02 us -> 4.8 us  [body(): weight = lax.all_gather(out_weight, 'dp', axis=0, tiled=True)]
    unnamed x6 -> x0, other arithmetic: 4.7 us -> none
    unnamed x50 -> x46, local copies, waits for them, and re-layouts: 6.88 us -> 4.87 us
    all_to_all x2 -> x1, waiting for transfers between devices: 11 us -> 12.6 us  [body(): lax.all_to_all(prefix, 'sp', split_axis=0, concat_axis=0, tiled=True)]
    pallas_call x1 -> x2, Pallas kernels: 5.65 us -> 5.86 us  [the longest x1 4.87 us: body(): pl.pallas_call(lambda *refs: block_kernel(*refs, groups=groups, local=loc...]
  transfers between devices with their start and end apart: 5 -> 4, of which waited for: 3 -> 4; matrix products, arithmetic and copies ran while one was open for 7% -> 4% of each run, Pallas kernels for 3% -> 4%
where the time goes in v2:
time: 203 us; the launch traced here: 202 us
  blocking collectives  74.6 us (37%)
  waiting for transfers between devices  62.2 us (31%)
  matrix products  25.9 us (13%)
  between operations  13.7 us (7%)
  starting transfers between devices  12.2 us (6%)
  Pallas kernels  7.34 us (4%)
  local copies, waits for them, and re-layouts  6.2 us (3%)
    all_to_all x1, blocking collectives, body(): lax.all_to_all(outgoing.reshape(experts, slots, model), ('sp', 'dp'), spl...  53.2 us
    all_to_all x1, waiting for transfers between devices, body(): lax.all_to_all(done.reshape(experts, slots, model), ('sp', 'dp'), split_a...  42.5 us
    all_to_all x1, blocking collectives, body(): lax.all_to_all(states, 'sp', split_axis=0, concat_axis=0, tiled=True)  21.4 us
    all_to_all x1, waiting for transfers between devices, body(): lax.all_to_all(prefix, 'sp', split_axis=0, concat_axis=0, tiled=True)  12.6 us
    dot_general x1, matrix products, body(): jnp.dot(hidden, expert_down[0], preferred_element_type=F32).astype(BF16)  5.96 us
    ppermute x1, starting transfers between devices, body(): halo = lax.ppermute(tail, 'sp', [(i, i + 1) for i in range(ways - 1)])  4.9 us
    unnamed x46, local copies, waits for them, and re-layouts  4.87 us
    pallas_call x1, Pallas kernels, body(): pl.pallas_call(lambda *refs: block_kernel(*refs, groups=groups, local=loc...  4.87 us
  transfers between devices with their start and end apart: 4, of which 4 were waited for; matrix products, arithmetic and copies ran while one was open for 4% of the time, Pallas kernels for 4%

profile of v2, /device:TPU:0, one launch (start us, length us, event | category | flops | bytes accessed | tf_op | source)
XLA Modules:
  0.0 202.2 jit_solution(4572871299217062509)
XLA Ops:
  8.4 4.9 %collective-permute-start = (bf16[8,4096]{1,0:T(8,128)(2,1)S(1)}, bf16[8,4096]{1,0:T(8,128)(2,1)S(1)}, u32[]{:S(2)}, u32[]{:S(2)}) collective-permute-start(bf16[8,4096]{1,0:T(8,128)(2,1)S(1)} %pad_maximum_fusion), channel_id=1, source_target_pairs={{0,4},{4,8},{8,12},{12,16},{16,20},{20,24},{24,28},{1,5},{5,9},{9,... | collective-permute-start | bytes 196616 | tf_op jit(solution)/shard_map/ppermute | solution.py:169
  13.6 1.6 collective-permute-done.refs_3_
  15.2 0.9 copy-done.7
  16.2 4.9 %shard_map.217 = (f32[128,2048]{1,0:T(8,128)S(1)}, bf16[128,1024]{1,0:T(8,128)(2,1)S(1)}, f32[128,32]{1,0:T(8,128)S(1)}, bf16[8,272,128]{2,1,0:T(8,128)(2,1)S(1)}) custom-call(bf16[128,2048]{1,0:T(8,128)(2,1)S(1)} %bitcast.59, bf16[128,1024]{1,0:T(8,128)(2,1)S(1)} %bitcast.60, bf16[128,1024]{1,0:T(8,128)(2,1)S(1)} %bitcast.61, ...), custom_call_target="tpu_custom_call" | custom-call | flops 400000000 | bytes 5000000 | tf_op jit(solution)/shard_map/pallas_call | solution.py:170
  21.0 1.0 copy-done.1
  22.1 21.4 %all_to_all.20.refs_0_ = bf16[8,272,128]{2,1,0:T(8,128)(2,1)S(1)} all-to-all(bf16[8,272,128]{2,1,0:T(8,128)(2,1)S(1)} %get-tuple-element.12), channel_id=1, replica_groups=mesh['sp'=8,'dp'=4] {'sp'}, dimensions={0} | all-to-all | bytes 1114112 | tf_op jit(solution)/shard_map/all_to_all | solution.py:186
  43.5 1.0 shard_map.218
  44.5 3.5 %all-to-all-start.1 = ((bf16[8,256,128]{2,1,0:T(8,128)(2,1)}), bf16[8,256,128]{2,1,0:T(8,128)(2,1)S(1)}, u32[]{:S(2)}, u32[]{:S(2)}) async-start(bf16[8,256,128]{2,1,0:T(8,128)(2,1)} %shard_map.218), calls=%async_computation.1 | async-start | bytes 1048576 | tf_op jit(solution)/shard_map/all_to_all | solution.py:195
  48.8 12.6 %all-to-all-done.1 = bf16[8,256,128]{2,1,0:T(8,128)(2,1)S(1)} async-done(((bf16[8,256,128]{2,1,0:T(8,128)(2,1)}), bf16[8,256,128]{2,1,0:T(8,128)(2,1)S(1)}, u32[]{:S(2)}, u32[]{:S(2)}) %all-to-all-start.1) | async-done | bytes 524320 | tf_op jit(solution)/shard_map/all_to_all | solution.py:195
  61.4 1.2 copy-done.2
  62.6 1.0 copy-done.3
  63.7 1.5 shard_map.219
  65.2 4.8 %all-gather.2.cloned.1.call-done = bf16[2048,2048]{1,0:T(8,128)(2,1)} async-done(((bf16[512,2048]{1,0:T(8,128)(2,1)}), bf16[2048,2048]{1,0:T(8,128)(2,1)}) %all-gather.2.cloned.1.call-update) | async-done | bytes 8388624 | tf_op jit(solution)/shard_map/all_gather | solution.py:167
  70.0 4.8 %multiply_reduce_fusion = (f32[128]{0:T(128)S(1)}, f32[128,2048]{1,0:T(8,128)S(1)}) fusion(bf16[128,2048]{1,0:T(8,128)(2,1)S(1)} %shard_map.219, bf16[2048,2048]{1,0:T(8,128)(2,1)} %all-gather.2.cloned.1.call-done, bf16[1,128,2048]{2,1,0:T(8,128)(2,1)} %param.23), kind=kOutput, calls=%fused_computation.22 | convolution fusion | flops 1075314560 | bytes 10486272 | tf_op jit(solution)/shard_map/dot_general | solution.py:205
  74.8 0.8 convolution_convert_fusion
  75.6 53.2 %all_to_all.21 = bf16[32,16,2048]{2,1,0:T(8,128)(2,1)} all-to-all(bf16[32,16,2048]{2,1,0:T(8,128)(2,1)S(1)} %bitcast.64), channel_id=1, replica_groups=mesh['sp'=8,'dp'=4] {'sp','dp'}, dimensions={0} | all-to-all | bytes 4194304 | tf_op jit(solution)/shard_map/all_to_all | solution.py:232
  128.9 2.8 %fusion.8 = f32[512,512]{1,0:T(8,128)S(1)} fusion(bf16[512,2048]{1,0:T(8,128)(2,1)} %bitcast.18, bf16[1,2048,512]{2,1,0:T(8,128)(2,1)S(1)} %copy-done.21), kind=kOutput, calls=%fused_computation.13 | convolution fusion | flops 1073741824 | bytes 5242880 | tf_op jit(solution)/shard_map/dot_general | solution.py:239
  131.7 6.0 %convolution_convert_fusion.1 = bf16[512,2048]{1,0:T(8,128)(2,1)} fusion(bf16[1,512,2048]{2,1,0:T(8,128)(2,1)S(1)} %copy-done, bf16[512,2048]{1,0:T(8,128)(2,1)} %bitcast.18, bf16[1,2048,512]{2,1,0:T(8,128)(2,1)} %param.42, f32[512,512]{1,0:T(8,128)S(1)} %fusion.8), kind=kOutput, calls=%fused_computation.1 | convolution fusion | flops 2150105088 | bytes 9437184 | tf_op jit(solution)/shard_map/dot_general | solution.py:242
  137.7 3.8 %all-to-all-start.3 = ((bf16[32,16,2048]{2,1,0:T(8,128)(2,1)}), bf16[32,16,2048]{2,1,0:T(8,128)(2,1)}, u32[]{:S(2)}, u32[]{:S(2)}) async-start(bf16[32,16,2048]{2,1,0:T(8,128)(2,1)} %bitcast.65), calls=%async_computation.3 | async-start | bytes 4194304 | tf_op jit(solution)/shard_map/all_to_all | solution.py:248
  141.5 2.1 %fusion.49 = f32[128,512]{1,0:T(8,128)S(1)} fusion(bf16[2048,512]{1,0:T(8,128)(2,1)} %param.38, f32[128,2048]{1,0:T(8,128)S(1)} %copy-done.14, f32[2048]{0:T(1024)S(1)} %copy-done.16, f32[128]{0:T(128)S(1)} %add_rsqrt_fusion), kind=kOutput, calls=%fused_computation.66 | convolution fusion | flops 269221888 | bytes 3416576 | tf_op jit(solution)/shard_map/dot_general | solution.py:252
  143.6 4.1 %convolution_add_fusion.1 = f32[128,2048]{1,0:T(8,128)} fusion(f32[128,2048]{1,0:T(8,128)S(1)} %copy-done.14, bf16[512,2048]{1,0:T(8,128)(2,1)} %param.40, bf16[2048,512]{1,0:T(8,128)(2,1)} %param.39, f32[128,512]{1,0:T(8,128)S(1)} %fusion.49, f32[2048]{0:T(1024)S(1)} %copy-done.16, f32[128]{0:T(128)S(1)} %add_rsqrt_fusion), kind=kOutput, calls=%fused_computation.4 | convolution fusion | flops 538312704 | bytes 6562304 | tf_op jit(solution)/shard_map/dot_general | solution.py:255
  147.7 42.5 %all-to-all-done.3 = bf16[32,16,2048]{2,1,0:T(8,128)(2,1)} async-done(((bf16[32,16,2048]{2,1,0:T(8,128)(2,1)}), bf16[32,16,2048]{2,1,0:T(8,128)(2,1)}, u32[]{:S(2)}, u32[]{:S(2)}) %all-to-all-start.3) | async-done | bytes 2097184 | tf_op jit(solution)/shard_map/all_to_all | solution.py:248
  190.2 2.1 %fusion.41 = f32[128,2048]{1,0:T(8,128)S(1)} fusion(bf16[512,2048]{1,0:T(8,128)(2,1)} %bitcast.23, f32[128]{0:T(128)S(1)} %get-tuple-element.16, s32[128]{0:T(128)S(1)} %get-tuple-element.14, f32[128]{0:T(128)S(1)} %get-tuple-element.15, s32[128]{0:T(128)S(1)} %get-tuple-element.13), kind=kOutput, calls=%fused_computation.48 | convolution fusion | flops 268828672 | bytes 3147776 | tf_op jit(solution)/shard_map/dot_general | solution.py:256
  192.3 3.0 %fusion.4 = bf16[1,128,2048]{2,1,0:T(8,128)(2,1)} fusion(f32[128,2048]{1,0:T(8,128)S(1)} %copy-done.15, f32[128,2048]{1,0:T(8,128)S(1)} %fusion.41, bf16[512,2048]{1,0:T(8,128)(2,1)} %bitcast.23, f32[128]{0:T(128)S(1)} %get-tuple-element.16, s32[128]{0:T(128)S(1)} %get-tuple-element.14, f32[128]{0:T(128)S(1)} %get-tuple-element.15, s32[128]{0:T(128)S(1)} %get-tuple-element.13), kind=kOutput, calls=%fused_computation.9 | convolution fusion | flops 269811712 | bytes 4720640 | tf_op jit(solution)/shard_map/dot_general | solution.py:256
  (57 shorter events, 2.9 us)
Async XLA Ops:
  6.5 125.2 %copy-start = (bf16[1,512,2048]{2,1,0:T(8,128)(2,1)S(1)}, bf16[1,512,2048]{2,1,0:T(8,128)(2,1)}, u32[]{:S(2)}) copy-start(bf16[1,512,2048]{2,1,0:T(8,128)(2,1)} %param.43) | copy-start | bytes 6291460
  6.5 1.1 copy-start.6
  6.5 1.8 copy-start.5
  6.5 6.8 %copy-start.17 = (bf16[1,128,32]{1,2,0:T(8,128)(2,1)S(1)}, bf16[1,128,32]{1,2,0:T(8,128)(2,1)}, u32[]{:S(2)}) copy-start(bf16[1,128,32]{1,2,0:T(8,128)(2,1)} %param.28) | copy-start | bytes 24580
  6.5 6.9 %copy-start.20 = (f32[32]{0:T(128)S(1)}, f32[32]{0:T(128)}, u32[]{:S(2)}) copy-start(f32[32]{0:T(128)} %param.34) | copy-start | bytes 388
  6.5 8.6 %copy-start.11 = (f32[32]{0:T(128)S(1)}, f32[32]{0:T(128)}, u32[]{:S(2)}) copy-start(f32[32]{0:T(128)} %param.32) | copy-start | bytes 388
  6.6 8.6 %copy-start.12 = (f32[32]{0:T(128)S(1)}, f32[32]{0:T(128)}, u32[]{:S(2)}) copy-start(f32[32]{0:T(128)} %param.33) | copy-start | bytes 388
  6.6 8.6 %copy-start.8 = (bf16[4,2048]{1,0:T(4,128)(2,1)S(1)}, bf16[4,2048]{1,0:T(4,128)(2,1)}, u32[]{:S(2)}) copy-start(bf16[4,2048]{1,0:T(4,128)(2,1)} %refs_5_.1) | copy-start | bytes 49156
  6.6 8.6 %copy-start.9 = (bf16[4,1024]{1,0:T(4,128)(2,1)S(1)}, bf16[4,1024]{1,0:T(4,128)(2,1)}, u32[]{:S(2)}) copy-start(bf16[4,1024]{1,0:T(4,128)(2,1)} %refs_6_.1) | copy-start | bytes 24580
  6.6 8.6 %copy-start.10 = (bf16[4,1024]{1,0:T(4,128)(2,1)S(1)}, bf16[4,1024]{1,0:T(4,128)(2,1)}, u32[]{:S(2)}) copy-start(bf16[4,1024]{1,0:T(4,128)(2,1)} %refs_7_.1) | copy-start | bytes 24580
  6.6 63.4 %all-gather.2.cloned.1.call-start = ((), (), s32[]{:S(2)}) async-start(), calls=%async_computation.4 | async-start | bytes 10485760 | tf_op jit(solution)/shard_map/all_gather | solution.py:167
  8.4 6.8 %collective-permute-start = (bf16[8,4096]{1,0:T(8,128)(2,1)S(1)}, bf16[8,4096]{1,0:T(8,128)(2,1)S(1)}, u32[]{:S(2)}, u32[]{:S(2)}) collective-permute-start(bf16[8,4096]{1,0:T(8,128)(2,1)S(1)} %pad_maximum_fusion), channel_id=1, source_target_pairs={{0,4},{4,8},{8,12},{12,16},{16,20},{20,24},{24,28},{1,5},{5,9},{9,... | collective-permute-start | bytes 196616 | tf_op jit(solution)/shard_map/ppermute | solution.py:169
  21.0 1.1 copy-start.1
  22.1 25.9 %copy-start.18 = (s32[1,128,2]{1,2,0:T(2,128)S(1)}, s32[1,128,2]{1,2,0:T(2,128)}, u32[]{:S(2)}) copy-start(s32[1,128,2]{1,2,0:T(2,128)} %param.44) | copy-start | bytes 3076
  22.1 39.3 %copy-start.4 = (f32[2048]{0:T(1024)S(1)}, f32[2048]{0:T(1024)}, u32[]{:S(2)}) copy-start(f32[2048]{0:T(1024)} %param.35) | copy-start | bytes 24580
  44.5 16.9 %all-to-all-start.1 = ((bf16[8,256,128]{2,1,0:T(8,128)(2,1)}), bf16[8,256,128]{2,1,0:T(8,128)(2,1)S(1)}, u32[]{:S(2)}, u32[]{:S(2)}) async-start(bf16[8,256,128]{2,1,0:T(8,128)(2,1)} %shard_map.218), calls=%async_computation.1 | async-start | bytes 1048576 | tf_op jit(solution)/shard_map/all_to_all | solution.py:195
  61.4 1.2 copy-start.2
  65.2 9.7 %copy-start.16 = (f32[2048]{0:T(1024)S(1)}, f32[2048]{0:T(1024)}, u32[]{:S(2)}) copy-start(f32[2048]{0:T(1024)} %param.37) | copy-start | bytes 24580
  74.8 54.1 %copy-start.13 = (f32[128,2048]{1,0:T(8,128)}, f32[128,2048]{1,0:T(8,128)S(1)}, u32[]{:S(2)}) copy-start(f32[128,2048]{1,0:T(8,128)S(1)} %get-tuple-element.18) | copy-start | bytes 3145732
  75.6 53.2 %copy-start.21 = (bf16[1,2048,512]{2,1,0:T(8,128)(2,1)S(1)}, bf16[1,2048,512]{2,1,0:T(8,128)(2,1)}, u32[]{:S(2)}) copy-start(bf16[1,2048,512]{2,1,0:T(8,128)(2,1)} %param.41) | copy-start | bytes 6291460
  137.7 3.8 %copy-start.19 = (f32[1,128,2]{1,2,0:T(2,128)S(1)}, f32[1,128,2]{1,2,0:T(2,128)}, u32[]{:S(2)}) copy-start(f32[1,128,2]{1,2,0:T(2,128)} %param.45) | copy-start | bytes 3076
  137.7 3.8 %copy-start.14 = (f32[128,2048]{1,0:T(8,128)S(1)}, f32[128,2048]{1,0:T(8,128)}, u32[]{:S(2)}) copy-start(f32[128,2048]{1,0:T(8,128)} %copy-done.13) | copy-start | bytes 3145732
  137.7 52.5 %all-to-all-start.3 = ((bf16[32,16,2048]{2,1,0:T(8,128)(2,1)}), bf16[32,16,2048]{2,1,0:T(8,128)(2,1)}, u32[]{:S(2)}, u32[]{:S(2)}) async-start(bf16[32,16,2048]{2,1,0:T(8,128)(2,1)} %bitcast.65), calls=%async_computation.3 | async-start | bytes 4194304 | tf_op jit(solution)/shard_map/all_to_all | solution.py:248
  147.7 44.6 %copy-start.15 = (f32[128,2048]{1,0:T(8,128)S(1)}, f32[128,2048]{1,0:T(8,128)}, u32[]{:S(2)}) copy-start(f32[128,2048]{1,0:T(8,128)} %convolution_add_fusion.1) | copy-start | bytes 3145732
  (2 other events, 2.0 us)
Sparse Core Ops, SparseCore 0:
  9.0 60.9 all-gather.1
